TPU v7x, 128 devices: a whole 4x4x4 slice. The times are simulated.
128 devices in a mesh: fs: 32 (over z, y, core), tp: 4 (over x).
Axes of the slice: x: 4, y: 4, z: 4, core: 2. Of those that a mesh axis runs over, the one named last changes fastest.
Arguments:
- first_map: bfloat16 [24576, 2048], P('fs', 'tp'), may hold values from -6 to 6
- second_map: bfloat16 [24576, 2048], P('fs', 'tp'), may hold values from -6 to 6
- lambda_head: float32 [16], P('tp'), may hold values from 0.3 to 0.8
- head_gain: float32 [2048], P('tp'), may hold values from 0.1 to 1.9
- cot_output: bfloat16 [24576, 4096], P('fs'), may hold values from -6 to 6
- layer_input: bfloat16 [24576, 4096], P('fs'), may hold values from -6 to 6
- cot_values: bfloat16 [24576, 2048], P('fs', 'tp'), may hold values from -16 to 16
- factor_value: bfloat16 [4096, 256], P('fs'), may hold values from -1 to 1
- factor_output: bfloat16 [4096, 256], P('fs'), may hold values from -1 to 1
- weight_value: float32 [4096, 2048], P('fs', 'tp'), may hold values from -6 to 6
- weight_output: float32 [2048, 4096], P('tp', 'fs'), may hold values from -6 to 6
- first_value: float32 [256, 2048], P('fs', 'tp'), may hold values from -6 to 6
- second_value: float32 [256, 2048], P('fs', 'tp'), may hold values from 0.05 to 1
- first_output: float32 [256, 2048], P('fs', 'tp'), may hold values from -6 to 6
- second_output: float32 [256, 2048], P('fs', 'tp'), may hold values from 0.05 to 1
Outputs:
- new_weight_value: float32 [4096, 2048], P('fs', 'tp')
- new_first_value: float32 [256, 2048], P('fs', 'tp')
- new_second_value: float32 [256, 2048], P('fs', 'tp')
- copy_value: bfloat16 [4096, 2048], P(None, 'tp')
- new_weight_output: float32 [2048, 4096], P('tp', 'fs')
- new_first_output: float32 [256, 2048], P('fs', 'tp')
- new_second_output: float32 [256, 2048], P('fs', 'tp')
- copy_output: bfloat16 [2048, 4096], P('tp')
All inputs are finite; a program needn't handle non-finite values.
Results may differ from a plain program's by a relative error of at most 0.002.
Values may be sent and summed in bfloat16 or wider, within the bound.
A program may use at most 128 MiB of HBM per device.

v0:
```python
import math
import jax
import jax.numpy as jnp
from jax import lax
from jax.sharding import Mesh
from jax.sharding import PartitionSpec as P

RANK = 256
HV = 2048
FS = ("fs_0", "fs_1", "fs_2")
FS_TP = ("fs_0", "fs_1", "fs_2", "tp")
norm_epsilon = 1e-06
first_decay = 0.9
second_decay = 0.95
learn_rate = 0.1


def in_blocks(value, dim, devices):
    dims = value.shape
    tiles = value.reshape(*dims[:dim], devices, dims[dim] // devices, *dims[dim + 1 :])
    return jnp.moveaxis(tiles, dim, 0)


def sent_and_summed(value, axis, dim):
    devices = lax.axis_size(axis)
    tiles = lax.all_to_all(in_blocks(value, dim, devices), axis, 0, 0, tiled=True)
    return jnp.sum(tiles, axis=0)


def side_by_side(arrays, axis, dim, along):
    ends, at = ([], 0)
    for a in arrays[:-1]:
        at += a.shape[along]
        ends.append(at)
    both = jnp.concatenate(arrays, axis=along)
    return tuple(jnp.split(lax.all_gather(both, axis, axis=dim, tiled=True), ends, axis=along))


def over_axes(value, axes):
    for axis in axes:
        value = lax.psum(value, axis)
    return value


def gather_turned(arrays, axis, dims):
    turned = [jnp.moveaxis(a, dim, 0) for a, dim in zip(arrays, dims)]
    both = jnp.concatenate([t.reshape(len(t), -1) for t in turned], axis=1)
    result, at, outs = (lax.all_gather(both, axis, axis=0, tiled=True), 0, [])
    for t, dim in zip(turned, dims):
        slab = result[:, at : at + t[0].size].reshape(-1, *t.shape[1:])
        outs.append(jnp.moveaxis(slab, 0, dim))
        at += t[0].size
    return tuple(outs)


def head_output(first_map, second_map, lambda_head, head_gain):
    heads_here = lambda_head.shape[0]
    head_width = first_map.shape[1] // heads_here
    count_rows = first_map.shape[0]
    spread = jnp.repeat(lambda_head, head_width)
    differ = first_map.astype(jnp.float32) - spread[None, :] * second_map.astype(jnp.float32)
    grouped = differ.reshape(count_rows, heads_here, head_width)
    scaled = grouped * lax.rsqrt(jnp.mean(grouped * grouped, -1, keepdims=True) + norm_epsilon)
    return (scaled.reshape(count_rows, heads_here * head_width) * head_gain[None, :]).astype(
        jnp.bfloat16
    )


def moments(projected, clip_factor, first_old, second_old):
    scaled = clip_factor * projected
    first_new = first_decay * first_old + (1.0 - first_decay) * scaled
    second_new = second_decay * second_old + (1.0 - second_decay) * scaled * scaled
    return (first_new, second_new, first_new * lax.rsqrt(second_new))


def low_rank(left, right):
    return sent_and_summed(
        lax.dot_general(
            left,
            right,
            (((0,), (0,)), ((), ())),
            precision=lax.Precision.HIGHEST,
            preferred_element_type=jnp.float32,
        ),
        FS,
        0,
    )


def shards(
    first_map,
    second_map,
    lambda_head,
    head_gain,
    cot_output,
    layer_input,
    cot_values,
    factor_value,
    factor_output,
    weight_value,
    weight_output,
    first_value,
    second_value,
    first_output,
    second_output,
):
    heads_out = head_output(first_map, second_map, lambda_head, head_gain)
    factor_v32 = factor_value.astype(jnp.float32)
    factor_o32 = factor_output.astype(jnp.float32)
    whole_value, whole_output = side_by_side((factor_value, factor_output), FS, 0, 1)
    mapped_value = jnp.dot(layer_input, whole_value, preferred_element_type=jnp.float32)
    mapped_output = jnp.dot(cot_output, whole_output, preferred_element_type=jnp.float32)
    low_value = low_rank(mapped_value, cot_values.astype(jnp.float32))
    low_output = low_rank(mapped_output, heads_out.astype(jnp.float32))
    partial_value = jnp.sum(low_value * low_value) + jnp.sum(low_output * low_output)
    total = over_axes(partial_value, FS_TP)
    clip_factor = jnp.minimum(1.0, math.sqrt(RANK * HV) * lax.rsqrt(total + norm_epsilon))
    first_v, second_v, ratio_value = moments(low_value, clip_factor, first_value, second_value)
    first_o, second_o, ratio_output = moments(low_output, clip_factor, first_output, second_output)
    pieces = side_by_side((ratio_value, ratio_output), FS, 0, 1)
    added_value = jnp.dot(
        factor_v32, pieces[0], precision=lax.Precision.HIGHEST, preferred_element_type=jnp.float32
    )
    added_output = lax.dot_general(
        pieces[1],
        factor_o32,
        (((0,), (1,)), ((), ())),
        precision=lax.Precision.HIGHEST,
        preferred_element_type=jnp.float32,
    )
    new_value = weight_value - learn_rate * added_value
    new_output = weight_output - learn_rate * added_output
    copy_value, copy_output = gather_turned(
        (new_value.astype(jnp.bfloat16), new_output.astype(jnp.bfloat16)), FS, (0, 1)
    )
    return (new_value, first_v, second_v, copy_value, new_output, first_o, second_o, copy_output)


def solution(mesh):
    torus = Mesh(mesh.devices.reshape(4, 4, 2, mesh.shape["tp"]), ("fs_0", "fs_1", "fs_2", "tp"))
    placed = (
        P(FS, "tp"),
        P(FS, "tp"),
        P("tp"),
        P("tp"),
        P(FS, None),
        P(FS, None),
        P(FS, "tp"),
        P(FS, None),
        P(FS, None),
        P(FS, "tp"),
        P("tp", FS),
        P(FS, "tp"),
        P(FS, "tp"),
        P(FS, "tp"),
        P(FS, "tp"),
    )
    return jax.shard_map(
        shards,
        mesh=torus,
        in_specs=placed,
        out_specs=(
            P(FS, "tp"),
            P(FS, "tp"),
            P(FS, "tp"),
            P(None, "tp"),
            P("tp", FS),
            P(FS, "tp"),
            P(FS, "tp"),
            P("tp", None),
        ),
        check_vma=False,
    )
```

profile of v0, /device:TPU:1, one launch (start us, length us, event | category | flops | bytes accessed | tf_op | source)
XLA Modules:
  0.0 256.5 jit_solution(15353092697436282198)
XLA Ops:
  7.2 0.0 copy-start
  7.2 0.0 all-gather.4.cloned.1.call-start
  7.2 1.6 pad_maximum_fusion.1
  8.8 0.0 all-gather.4.cloned.1.call-update
  8.9 0.7 broadcast_bitcast_fusion
  9.6 2.8 %fusion.6 = f32[768,512]{1,0:T(8,128)} fusion(bf16[768,512]{1,0:T(8,128)(2,1)} %param.16, bf16[768,512]{1,0:T(8,128)(2,1)} %param.15, f32[512]{0:T(512)S(1)} %broadcast_bitcast_fusion), kind=kLoop, calls=%fused_computation.9 | loop fusion | flops 1966080 | bytes 3147776 | tf_op jit(solution)/shard_map/mul | solution.py:63
  12.4 1.8 mul.106
  14.1 0.9 reduce_sum.47
  15.0 0.1 add_rsqrt_fusion
  15.1 45.5 %all-gather.4.cloned.1.call-done = bf16[4096,512]{1,0:T(8,128)(2,1)} async-done(((bf16[128,512]{1,0:T(8,128)(2,1)}), bf16[4096,512]{1,0:T(8,128)(2,1)}) %all-gather.4.cloned.1.call-update) | async-done | bytes 4194320 | tf_op jit(solution)/shard_map/all_gather | solution.py:36
  60.6 5.3 %fusion.2 = f32[256,768]{1,0:T(8,128)S(1)} fusion(bf16[768,4096]{1,0:T(8,128)(2,1)} %param.20, bf16[4096,512]{1,0:T(8,128)(2,1)} %all-gather.4.cloned.1.call-done), kind=kOutput, calls=%fused_computation.3 | convolution fusion | flops 1610612736 | bytes 9175040 | tf_op jit(solution)/shard_map/dot_general | solution.py:111
  65.9 1.6 convolution_bitcast_fusion
  67.5 5.3 %all-to-all-start = ((f32[32,8,512]{2,1,0:T(8,128)}), f32[32,8,512]{2,1,0:T(8,128)S(1)}, u32[]{:S(2)}, u32[]{:S(2)}) async-start(f32[32,8,512]{2,1,0:T(8,128)} %convolution_bitcast_fusion), calls=%async_computation | async-start | bytes 1048576 | tf_op jit(solution)/shard_map/all_to_all | solution.py:26
  72.8 0.0 copy-start.12
  72.8 5.3 %fusion.7 = f32[32,8,768]{2,1,0:T(8,128)S(1)} fusion(bf16[768,4096]{1,0:T(8,128)(2,1)} %param.19, bf16[4096,512]{1,0:T(8,128)(2,1)} %all-gather.4.cloned.1.call-done), kind=kOutput, calls=%fused_computation.10 | convolution fusion | flops 1610612736 | bytes 9175040 | tf_op jit(solution)/shard_map/dot_general | solution.py:112
  78.1 0.0 copy-start.1
  78.1 0.0 copy-start.2
  78.1 1.0 mul.107
  79.1 0.1 copy-done.1
  79.2 0.2 copy-done.2
  79.5 1.8 fusion.14
  81.3 0.0 copy-start.5
  81.3 0.0 copy-start.7
  81.4 2.9 %all-to-all-done = f32[32,8,512]{2,1,0:T(8,128)S(1)} async-done(((f32[32,8,512]{2,1,0:T(8,128)}), f32[32,8,512]{2,1,0:T(8,128)S(1)}, u32[]{:S(2)}, u32[]{:S(2)}) %all-to-all-start) | async-done | bytes 524320 | tf_op jit(solution)/shard_map/all_to_all | solution.py:26
  84.2 4.6 %all-to-all-start.1 = ((f32[32,8,512]{2,1,0:T(8,128)}), f32[32,8,512]{2,1,0:T(8,128)S(1)}, u32[]{:S(2)}, u32[]{:S(2)}) async-start(f32[32,8,512]{2,1,0:T(8,128)} %fusion.14), calls=%async_computation.1 | async-start | bytes 1048576 | tf_op jit(solution)/shard_map/all_to_all | solution.py:26
  88.9 0.0 all-gather.6.cloned.1.call-start
  89.0 0.6 multiply_reduce_fusion.1
  89.6 10.7 %all-to-all-done.1 = f32[32,8,512]{2,1,0:T(8,128)S(1)} async-done(((f32[32,8,512]{2,1,0:T(8,128)}), f32[32,8,512]{2,1,0:T(8,128)S(1)}, u32[]{:S(2)}, u32[]{:S(2)}) %all-to-all-start.1) | async-done | bytes 524320 | tf_op jit(solution)/shard_map/all_to_all | solution.py:26
  100.4 0.6 multiply_reduce_fusion
  102.3 7.4 %psum.28 = f32[]{:T(128)} all-reduce(f32[]{:T(128)S(6)} %add.39), channel_id=1, replica_groups=mesh['fs_0'=4,'fs_1'=4,'fs_2'=2,'tp'=4] {'fs_0'}, use_global_device_ids=true, to_apply=%region_5.0 | all-reduce | flops 1 | bytes 8 | tf_op jit(solution)/shard_map/psum | solution.py:41
  109.6 8.4 %psum.29 = f32[]{:T(128)} all-reduce(f32[]{:T(128)} %psum.28), channel_id=1, replica_groups=mesh['fs_0'=4,'fs_1'=4,'fs_2'=2,'tp'=4] {'fs_1'}, use_global_device_ids=true, to_apply=%region_6.0 | all-reduce | flops 1 | bytes 8 | tf_op jit(solution)/shard_map/psum | solution.py:41
  118.1 5.8 %psum.30 = f32[]{:T(128)} all-reduce(f32[]{:T(128)} %psum.29), channel_id=1, replica_groups=mesh['fs_0'=4,'fs_1'=4,'fs_2'=2,'tp'=4] {'fs_2'}, use_global_device_ids=true, to_apply=%region_7.0 | all-reduce | flops 1 | bytes 8 | tf_op jit(solution)/shard_map/psum | solution.py:41
  123.9 9.0 %psum.31 = f32[]{:T(128)} all-reduce(f32[]{:T(128)} %psum.30), channel_id=1, replica_groups=mesh['fs_0'=4,'fs_1'=4,'fs_2'=2,'tp'=4] {'tp'}, use_global_device_ids=true, to_apply=%region_8.0 | all-reduce | flops 1 | bytes 8 | tf_op jit(solution)/shard_map/psum | solution.py:41
  133.6 0.6 rsqrt_multiply_fusion
  134.3 0.6 pad_maximum_fusion.2
  134.9 0.0 all-gather.6.cloned.1.call-update
  134.9 0.0 all-gather.8.cloned.1.call-start
  135.0 0.1 copy.32
  135.1 39.8 %all-gather.6.cloned.1.call-done = f32[256,1024]{1,0:T(8,128)} async-done(((f32[8,1024]{1,0:T(8,128)}), f32[256,1024]{1,0:T(8,128)}) %all-gather.6.cloned.1.call-update) | async-done | bytes 1048592 | tf_op jit(solution)/shard_map/all_gather | solution.py:36
  175.0 1.7 fusion.10
  176.6 0.0 copy-start.3
  176.7 1.7 fusion.24
  178.4 0.7 pad_maximum_fusion
  179.1 0.0 all-gather.8.cloned.1.call-update
  179.1 0.8 copy.33
  180.0 57.5 %all-gather.8.cloned.1.call-done = bf16[4096,1024]{0,1:T(8,128)(2,1)} async-done(((bf16[128,1024]{0,1:T(8,128)(2,1)}), bf16[4096,1024]{0,1:T(8,128)(2,1)}) %all-gather.8.cloned.1.call-update) | async-done | bytes 8388624 | tf_op jit(solution)/shard_map/all_gather | solution.py:48
  237.5 6.0 %slice_bitcast_fusion = (bf16[512,4096]{1,0:T(8,128)(2,1)}, bf16[4096,512]{0,1:T(8,128)(2,1)}) fusion(bf16[4096,1024]{0,1:T(8,128)(2,1)} %all-gather.8.cloned.1.call-done), kind=kLoop, calls=%fused_computation | loop fusion | bytes 16777216 | tf_op jit(solution)/shard_map/transpose | solution.py:51
  243.5 6.4 %copy.34 = bf16[4096,512]{1,0:T(8,128)(2,1)} copy(bf16[4096,512]{0,1:T(8,128)(2,1)} %get-tuple-element.39) | data formatting | bytes 8388608
  (20 shorter events, 0.1 us)
Async XLA Ops:
  7.2 58.7 %copy-start = (bf16[768,512]{1,0:T(8,128)(2,1)S(1)}, bf16[768,512]{1,0:T(8,128)(2,1)}, u32[]{:S(2)}) copy-start(bf16[768,512]{1,0:T(8,128)(2,1)} %param.21) | copy-start | bytes 2359300
  7.2 53.5 %all-gather.4.cloned.1.call-start = ((), (), s32[]{:S(2)}) async-start(), calls=%async_computation.2 | async-start | bytes 4325376 | tf_op jit(solution)/shard_map/all_gather | solution.py:36
  67.5 16.7 %all-to-all-start = ((f32[32,8,512]{2,1,0:T(8,128)}), f32[32,8,512]{2,1,0:T(8,128)S(1)}, u32[]{:S(2)}, u32[]{:S(2)}) async-start(f32[32,8,512]{2,1,0:T(8,128)} %convolution_bitcast_fusion), calls=%async_computation | async-start | bytes 1048576 | tf_op jit(solution)/shard_map/all_to_all | solution.py:26
  72.8 6.3 %copy-start.12 = (f32[512]{0:T(512)S(1)}, f32[512]{0:T(512)}, u32[]{:S(2)}) copy-start(f32[512]{0:T(512)} %param.18) | copy-start | bytes 6148
  78.1 1.1 copy-start.1
  78.1 1.4 copy-start.2
  81.3 52.3 %copy-start.8 = (f32[8,512]{1,0:T(8,128)S(1)}, f32[8,512]{1,0:T(8,128)}, u32[]{:S(2)}) copy-start(f32[8,512]{1,0:T(8,128)} %param.29) | copy-start | bytes 49156
  81.3 52.3 %copy-start.9 = (f32[8,512]{1,0:T(8,128)S(1)}, f32[8,512]{1,0:T(8,128)}, u32[]{:S(2)}) copy-start(f32[8,512]{1,0:T(8,128)} %param.28) | copy-start | bytes 49156
  81.3 52.3 %copy-start.10 = (f32[8,512]{1,0:T(8,128)S(1)}, f32[8,512]{1,0:T(8,128)}, u32[]{:S(2)}) copy-start(f32[8,512]{1,0:T(8,128)} %param.27) | copy-start | bytes 49156
  81.3 52.3 %copy-start.11 = (f32[8,512]{1,0:T(8,128)S(1)}, f32[8,512]{1,0:T(8,128)}, u32[]{:S(2)}) copy-start(f32[8,512]{1,0:T(8,128)} %param.26) | copy-start | bytes 49156
  81.3 53.7 %copy-start.5 = (f32[128,512]{1,0:T(8,128)S(1)}, f32[128,512]{1,0:T(8,128)}, u32[]{:S(2)}) copy-start(f32[128,512]{1,0:T(8,128)} %param.24) | copy-start | bytes 786436
  81.3 93.6 %copy-start.4 = (f32[512,128]{1,0:T(8,128)S(1)}, f32[512,128]{1,0:T(8,128)}, u32[]{:S(2)}) copy-start(f32[512,128]{1,0:T(8,128)} %param.25) | copy-start | bytes 786436
  81.3 93.6 %copy-start.6 = (bf16[128,256]{1,0:T(8,128)(2,1)S(1)}, bf16[128,256]{1,0:T(8,128)(2,1)}, u32[]{:S(2)}) copy-start(bf16[128,256]{1,0:T(8,128)(2,1)} %param.23) | copy-start | bytes 196612
  81.3 95.3 %copy-start.7 = (bf16[128,256]{1,0:T(8,128)(2,1)S(1)}, bf16[128,256]{1,0:T(8,128)(2,1)}, u32[]{:S(2)}) copy-start(bf16[128,256]{1,0:T(8,128)(2,1)} %param.22) | copy-start | bytes 196612
  84.2 16.1 %all-to-all-start.1 = ((f32[32,8,512]{2,1,0:T(8,128)}), f32[32,8,512]{2,1,0:T(8,128)S(1)}, u32[]{:S(2)}, u32[]{:S(2)}) async-start(f32[32,8,512]{2,1,0:T(8,128)} %fusion.14), calls=%async_computation.1 | async-start | bytes 1048576 | tf_op jit(solution)/shard_map/all_to_all | solution.py:26
  88.9 86.1 %all-gather.6.cloned.1.call-start = ((), (), s32[]{:S(2)}) async-start(), calls=%async_computation.3 | async-start | bytes 1081344 | tf_op jit(solution)/shard_map/all_gather | solution.py:36
  134.9 102.6 %all-gather.8.cloned.1.call-start = ((), (), s32[]{:S(2)}) async-start(), calls=%async_computation.4 | async-start | bytes 8650752 | tf_op jit(solution)/shard_map/all_gather | solution.py:48
  176.6 66.9 %copy-start.3 = (f32[512,128]{1,0:T(8,128)}, f32[512,128]{1,0:T(8,128)S(1)}, u32[]{:S(2)}) copy-start(f32[512,128]{1,0:T(8,128)S(1)} %fusion.10) | copy-start | bytes 786436
Sparse Core Ops, SparseCore 0:
  10.8 49.7 all-gather.3
  135.0 39.8 all-gather.5
  179.2 58.2 all-gather.7
where the time goes:
time: 257 us; the launch traced here: 256 us
  waiting for transfers between devices  157 us (61%)
  blocking collectives  30.6 us (12%)
  local copies, waits for them, and re-layouts  17.3 us (7%)
  matrix products  17.3 us (7%)
  between operations  16 us (6%)
  starting transfers between devices  10.1 us (4%)
  other arithmetic  8.61 us (3%)
    all_gather x2, waiting for transfers between devices, side_by_side(): lax.all_gather(both, axis, axis=dim, tiled=True)  85.4 us
    all_gather x1, waiting for transfers between devices, gather_turned(): result, at, outs = (lax.all_gather(both, axis, axis=0, tiled=True), 0, [])  57.5 us
    psum x4, blocking collectives, over_axes(): value = lax.psum(value, axis)  30.6 us
    all_to_all x2, waiting for transfers between devices, sent_and_summed(): lax.all_to_all(in_blocks(value, dim, devices), axis, 0, 0, tiled=True)  13.6 us
    all_to_all x2, starting transfers between devices, sent_and_summed(): lax.all_to_all(in_blocks(value, dim, devices), axis, 0, 0, tiled=True)  9.94 us
    unnamed x29, local copies, waits for them, and re-layouts  7.8 us
    transpose x1, local copies, waits for them, and re-layouts, gather_turned(): outs.append(jnp.moveaxis(slab, 0, dim))  6.03 us
    dot_general x1, matrix products, shards(): jnp.dot(cot_output, whole_output, preferred_element_type=jnp.float32)  5.27 us
  transfers between devices with their start and end apart: 5, of which 5 were waited for; matrix products, arithmetic and copies ran while one was open for 6% of the time, Pallas kernels for 0%

commit v1 on v0

--- a/solution.py
+++ b/solution.py
@@ -4,6 +4,7 @@
 from jax import lax
 from jax.sharding import Mesh
 from jax.sharding import PartitionSpec as P
+from jax.lax import all_to_all, axis_size
 
 RANK = 256
 HV = 2048
@@ -45,7 +46,16 @@
 def gather_turned(arrays, axis, dims):
     turned = [jnp.moveaxis(a, dim, 0) for a, dim in zip(arrays, dims)]
     both = jnp.concatenate([t.reshape(len(t), -1) for t in turned], axis=1)
-    result, at, outs = (lax.all_gather(both, axis, axis=0, tiled=True), 0, [])
+    result, at, outs = (
+        jnp.concatenate(
+            all_to_all(
+                jnp.stack([both] * axis_size(axis)), axis_name=axis, split_axis=0, concat_axis=0
+            ),
+            0,
+        ),
+        0,
+        [],
+    )
     for t, dim in zip(turned, dims):
         slab = result[:, at : at + t[0].size].reshape(-1, *t.shape[1:])
         outs.append(jnp.moveaxis(slab, 0, dim))

time: 257 us -> 326 us (1.27); the launches traced: 256 us -> 321 us
  waiting for transfers between devices: 157 us -> 199 us
  local copies, waits for them, and re-layouts: 17.3 us -> 34.2 us
  starting transfers between devices: 10.1 us -> 15.4 us
    all_to_all x0 -> x1, waiting for transfers between devices: none -> 99.9 us  [gather_turned(): all_to_all(jnp.stack([both] * axis_size(axis)), axis_name=axis, split_axi...]
    all_gather x1 -> x0, waiting for transfers between devices: 57.5 us -> none  [gather_turned(): result, at, outs = (lax.all_gather(both, axis, axis=0, tiled=True), 0, [])]
    all_to_all x0 -> x1, local copies, waits for them, and re-layouts: none -> 11.9 us  [gather_turned(): all_to_all(jnp.stack([both] * axis_size(axis)), axis_name=axis, split_axi...]
    all_to_all x0 -> x1, starting transfers between devices: none -> 5.35 us  [gather_turned(): all_to_all(jnp.stack([both] * axis_size(axis)), axis_name=axis, split_axi...]
    another operation x0 -> x1, local copies, waits for them, and re-layouts: none -> 5.11 us  [gather_turned(): jnp.stack([both] * axis_size(axis))]
    unnamed x29 -> x31, local copies, waits for them, and re-layouts: 7.8 us -> 7.8 us
  transfers between devices with their start and end apart: 5 -> 5, of which waited for: 5 -> 5; matrix products, arithmetic and copies ran while one was open for 6% -> 5% of each run, Pallas kernels for 0% -> 0%
where the time goes in v1:
time: 326 us; the launch traced here: 321 us
  waiting for transfers between devices  199 us (61%)
  local copies, waits for them, and re-layouts  34.2 us (10%)
  blocking collectives  30.6 us (9%)
  matrix products  17.3 us (5%)
  between operations  16.3 us (5%)
  starting transfers between devices  15.4 us (5%)
  other arithmetic  7.91 us (2%)
    all_to_all x1, waiting for transfers between devices, gather_turned(): all_to_all(jnp.stack([both] * axis_size(axis)), axis_name=axis, split_axi...  99.9 us
    all_gather x2, waiting for transfers between devices, side_by_side(): lax.all_gather(both, axis, axis=dim, tiled=True)  85.4 us
    psum x4, blocking collectives, over_axes(): value = lax.psum(value, axis)  30.6 us
    all_to_all x2, waiting for transfers between devices, sent_and_summed(): lax.all_to_all(in_blocks(value, dim, devices), axis, 0, 0, tiled=True)  13.6 us
    all_to_all x1, local copies, waits for them, and re-layouts, gather_turned(): all_to_all(jnp.stack([both] * axis_size(axis)), axis_name=axis, split_axi...  11.9 us
    all_to_all x2, starting transfers between devices, sent_and_summed(): lax.all_to_all(in_blocks(value, dim, devices), axis, 0, 0, tiled=True)  9.94 us
    unnamed x31, local copies, waits for them, and re-layouts  7.8 us
  transfers between devices with their start and end apart: 5, of which 5 were waited for; matrix products, arithmetic and copies ran while one was open for 5% of the time, Pallas kernels for 0%

profile of v1, /device:TPU:1, one launch (start us, length us, event | category | flops | bytes accessed | tf_op | source)
XLA Modules:
  0.0 320.6 jit_solution(10125278360068570692)
XLA Ops:
  7.2 0.0 copy-start
  7.2 0.0 all-gather.3.cloned.1.call-start
  7.2 1.6 pad_maximum_fusion.1
  8.8 0.0 all-gather.3.cloned.1.call-update
  8.9 0.7 broadcast_bitcast_fusion
  9.6 2.8 fusion.6
  12.4 1.8 mul.106
  14.2 0.9 reduce_sum.47
  15.0 0.1 add_rsqrt_fusion
  15.1 45.5 %all-gather.3.cloned.1.call-done = bf16[4096,512]{1,0:T(8,128)(2,1)} async-done(((bf16[128,512]{1,0:T(8,128)(2,1)}), bf16[4096,512]{1,0:T(8,128)(2,1)}) %all-gather.3.cloned.1.call-update) | async-done | bytes 4194320 | tf_op jit(solution)/shard_map/all_gather | solution.py:37
  60.6 5.3 %fusion.2 = f32[256,768]{1,0:T(8,128)S(1)} fusion(bf16[768,4096]{1,0:T(8,128)(2,1)} %param.20, bf16[4096,512]{1,0:T(8,128)(2,1)} %all-gather.3.cloned.1.call-done), kind=kOutput, calls=%fused_computation.3 | convolution fusion | flops 1610612736 | bytes 9175040 | tf_op jit(solution)/shard_map/dot_general | solution.py:121
  65.9 1.6 convolution_bitcast_fusion
  67.5 5.3 %all-to-all-start = ((f32[32,8,512]{2,1,0:T(8,128)}), f32[32,8,512]{2,1,0:T(8,128)S(1)}, u32[]{:S(2)}, u32[]{:S(2)}) async-start(f32[32,8,512]{2,1,0:T(8,128)} %convolution_bitcast_fusion), calls=%async_computation | async-start | bytes 1048576 | tf_op jit(solution)/shard_map/all_to_all | solution.py:27
  72.8 0.0 copy-start.13
  72.8 5.3 %fusion.7 = f32[32,8,768]{2,1,0:T(8,128)S(1)} fusion(bf16[768,4096]{1,0:T(8,128)(2,1)} %param.19, bf16[4096,512]{1,0:T(8,128)(2,1)} %all-gather.3.cloned.1.call-done), kind=kOutput, calls=%fused_computation.10 | convolution fusion | flops 1610612736 | bytes 9175040 | tf_op jit(solution)/shard_map/dot_general | solution.py:122
  78.1 0.0 copy-start.2
  78.1 0.0 copy-start.3
  78.1 1.0 mul.107
  79.1 0.1 copy-done.2
  79.2 0.2 copy-done.3
  79.5 1.8 fusion.14
  81.3 0.0 copy-start.6
  81.3 0.0 copy-start.8
  81.4 2.9 all-to-all-done
  84.2 4.6 %all-to-all-start.1 = ((f32[32,8,512]{2,1,0:T(8,128)}), f32[32,8,512]{2,1,0:T(8,128)S(1)}, u32[]{:S(2)}, u32[]{:S(2)}) async-start(f32[32,8,512]{2,1,0:T(8,128)} %fusion.14), calls=%async_computation.1 | async-start | bytes 1048576 | tf_op jit(solution)/shard_map/all_to_all | solution.py:27
  88.9 0.0 all-gather.5.cloned.1.call-start
  89.0 0.6 multiply_reduce_fusion.1
  89.6 10.7 %all-to-all-done.1 = f32[32,8,512]{2,1,0:T(8,128)S(1)} async-done(((f32[32,8,512]{2,1,0:T(8,128)}), f32[32,8,512]{2,1,0:T(8,128)S(1)}, u32[]{:S(2)}, u32[]{:S(2)}) %all-to-all-start.1) | async-done | bytes 524320 | tf_op jit(solution)/shard_map/all_to_all | solution.py:27
  100.4 0.6 multiply_reduce_fusion
  102.3 7.4 %psum.28 = f32[]{:T(128)} all-reduce(f32[]{:T(128)S(6)} %add.39), channel_id=1, replica_groups=mesh['fs_0'=4,'fs_1'=4,'fs_2'=2,'tp'=4] {'fs_0'}, use_global_device_ids=true, to_apply=%region_5.0 | all-reduce | flops 1 | bytes 8 | tf_op jit(solution)/shard_map/psum | solution.py:42
  109.6 8.4 %psum.29 = f32[]{:T(128)} all-reduce(f32[]{:T(128)} %psum.28), channel_id=1, replica_groups=mesh['fs_0'=4,'fs_1'=4,'fs_2'=2,'tp'=4] {'fs_1'}, use_global_device_ids=true, to_apply=%region_6.0 | all-reduce | flops 1 | bytes 8 | tf_op jit(solution)/shard_map/psum | solution.py:42
  118.1 5.8 %psum.30 = f32[]{:T(128)} all-reduce(f32[]{:T(128)} %psum.29), channel_id=1, replica_groups=mesh['fs_0'=4,'fs_1'=4,'fs_2'=2,'tp'=4] {'fs_2'}, use_global_device_ids=true, to_apply=%region_7.0 | all-reduce | flops 1 | bytes 8 | tf_op jit(solution)/shard_map/psum | solution.py:42
  123.9 9.0 %psum.31 = f32[]{:T(128)} all-reduce(f32[]{:T(128)} %psum.30), channel_id=1, replica_groups=mesh['fs_0'=4,'fs_1'=4,'fs_2'=2,'tp'=4] {'tp'}, use_global_device_ids=true, to_apply=%region_8.0 | all-reduce | flops 1 | bytes 8 | tf_op jit(solution)/shard_map/psum | solution.py:42
  133.6 0.6 rsqrt_multiply_fusion
  134.3 0.6 pad_maximum_fusion.2
  134.9 0.0 all-gather.5.cloned.1.call-update
  134.9 0.1 copy.40
  135.1 39.9 %all-gather.5.cloned.1.call-done = f32[256,1024]{1,0:T(8,128)} async-done(((f32[8,1024]{1,0:T(8,128)}), f32[256,1024]{1,0:T(8,128)}) %all-gather.5.cloned.1.call-update) | async-done | bytes 1048592 | tf_op jit(solution)/shard_map/all_gather | solution.py:37
  175.0 1.7 fusion.10
  176.6 0.0 copy-start.4
  176.7 1.7 fusion.24
  178.4 5.1 %stack.2 = bf16[32,128,1024]{1,2,0:T(8,128)(2,1)} broadcast(bf16[128,1024]{0,1:T(8,128)(2,1)S(1)} %pad_maximum_fusion), dimensions={1,2} | broadcast | bytes 8650752 | tf_op jit(solution)/shard_map/stack | solution.py:52
  183.5 5.3 %all-to-all-start.2 = ((bf16[32,128,1024]{1,2,0:T(8,128)(2,1)}), bf16[32,128,1024]{1,2,0:T(8,128)(2,1)}, u32[]{:S(2)}, u32[]{:S(2)}) async-start(bf16[32,128,1024]{1,2,0:T(8,128)(2,1)} %stack.2), calls=%async_computation.2 | async-start | bytes 16777216 | tf_op jit(solution)/shard_map/all_to_all | solution.py:51
  188.9 0.8 copy.42
  189.7 99.9 %all-to-all-done.2 = bf16[32,128,1024]{1,2,0:T(8,128)(2,1)} async-done(((bf16[32,128,1024]{1,2,0:T(8,128)(2,1)}), bf16[32,128,1024]{1,2,0:T(8,128)(2,1)}, u32[]{:S(2)}, u32[]{:S(2)}) %all-to-all-start.2) | async-done | bytes 8388640 | tf_op jit(solution)/shard_map/all_to_all | solution.py:51
  289.6 11.9 %copy.41 = bf16[32,128,1024]{2,1,0:T(8,128)(2,1)} copy(bf16[32,128,1024]{1,2,0:T(8,128)(2,1)} %all-to-all-done.2) | data formatting | bytes 16777216 | tf_op jit(solution)/shard_map/all_to_all | solution.py:51
  301.5 5.8 %slice_bitcast_fusion = (bf16[512,4096]{0,1:T(8,128)(2,1)}, bf16[4096,512]{1,0:T(8,128)(2,1)}) fusion(bf16[4096,1024]{1,0:T(8,128)(2,1)} %bitcast.35), kind=kLoop, calls=%fused_computation | loop fusion | bytes 16777216 | tf_op jit(solution)/shard_map/transpose | solution.py:61
  307.4 6.4 %copy.43 = bf16[512,4096]{1,0:T(8,128)(2,1)} copy(bf16[512,4096]{0,1:T(8,128)(2,1)} %get-tuple-element.54) | data formatting | bytes 8388608
  (23 shorter events, 0.2 us)
Async XLA Ops:
  7.2 58.8 %copy-start = (bf16[768,512]{1,0:T(8,128)(2,1)S(1)}, bf16[768,512]{1,0:T(8,128)(2,1)}, u32[]{:S(2)}) copy-start(bf16[768,512]{1,0:T(8,128)(2,1)} %param.21) | copy-start | bytes 2359300
  7.2 53.5 %all-gather.3.cloned.1.call-start = ((), (), s32[]{:S(2)}) async-start(), calls=%async_computation.3 | async-start | bytes 4325376 | tf_op jit(solution)/shard_map/all_gather | solution.py:37
  67.5 16.7 %all-to-all-start = ((f32[32,8,512]{2,1,0:T(8,128)}), f32[32,8,512]{2,1,0:T(8,128)S(1)}, u32[]{:S(2)}, u32[]{:S(2)}) async-start(f32[32,8,512]{2,1,0:T(8,128)} %convolution_bitcast_fusion), calls=%async_computation | async-start | bytes 1048576 | tf_op jit(solution)/shard_map/all_to_all | solution.py:27
  72.8 6.3 %copy-start.13 = (f32[512]{0:T(512)S(1)}, f32[512]{0:T(512)}, u32[]{:S(2)}) copy-start(f32[512]{0:T(512)} %param.18) | copy-start | bytes 6148
  78.1 1.1 copy-start.2
  78.1 1.4 copy-start.3
  81.3 52.3 %copy-start.9 = (f32[8,512]{1,0:T(8,128)S(1)}, f32[8,512]{1,0:T(8,128)}, u32[]{:S(2)}) copy-start(f32[8,512]{1,0:T(8,128)} %param.29) | copy-start | bytes 49156
  81.3 52.3 %copy-start.10 = (f32[8,512]{1,0:T(8,128)S(1)}, f32[8,512]{1,0:T(8,128)}, u32[]{:S(2)}) copy-start(f32[8,512]{1,0:T(8,128)} %param.28) | copy-start | bytes 49156
  81.3 52.3 %copy-start.11 = (f32[8,512]{1,0:T(8,128)S(1)}, f32[8,512]{1,0:T(8,128)}, u32[]{:S(2)}) copy-start(f32[8,512]{1,0:T(8,128)} %param.27) | copy-start | bytes 49156
  81.3 52.3 %copy-start.12 = (f32[8,512]{1,0:T(8,128)S(1)}, f32[8,512]{1,0:T(8,128)}, u32[]{:S(2)}) copy-start(f32[8,512]{1,0:T(8,128)} %param.26) | copy-start | bytes 49156
  81.3 53.6 %copy-start.6 = (f32[128,512]{1,0:T(8,128)S(1)}, f32[128,512]{1,0:T(8,128)}, u32[]{:S(2)}) copy-start(f32[128,512]{1,0:T(8,128)} %param.24) | copy-start | bytes 786436
  81.3 93.6 %copy-start.5 = (f32[512,128]{1,0:T(8,128)S(1)}, f32[512,128]{1,0:T(8,128)}, u32[]{:S(2)}) copy-start(f32[512,128]{1,0:T(8,128)} %param.25) | copy-start | bytes 786436
  81.3 93.6 %copy-start.7 = (bf16[128,256]{1,0:T(8,128)(2,1)S(1)}, bf16[128,256]{1,0:T(8,128)(2,1)}, u32[]{:S(2)}) copy-start(bf16[128,256]{1,0:T(8,128)(2,1)} %param.23) | copy-start | bytes 196612
  81.3 95.3 %copy-start.8 = (bf16[128,256]{1,0:T(8,128)(2,1)S(1)}, bf16[128,256]{1,0:T(8,128)(2,1)}, u32[]{:S(2)}) copy-start(bf16[128,256]{1,0:T(8,128)(2,1)} %param.22) | copy-start | bytes 196612
  84.2 16.1 %all-to-all-start.1 = ((f32[32,8,512]{2,1,0:T(8,128)}), f32[32,8,512]{2,1,0:T(8,128)S(1)}, u32[]{:S(2)}, u32[]{:S(2)}) async-start(f32[32,8,512]{2,1,0:T(8,128)} %fusion.14), calls=%async_computation.1 | async-start | bytes 1048576 | tf_op jit(solution)/shard_map/all_to_all | solution.py:27
  88.9 86.1 %all-gather.5.cloned.1.call-start = ((), (), s32[]{:S(2)}) async-start(), calls=%async_computation.4 | async-start | bytes 1081344 | tf_op jit(solution)/shard_map/all_gather | solution.py:37
  176.6 6.9 %copy-start.4 = (f32[512,128]{1,0:T(8,128)}, f32[512,128]{1,0:T(8,128)S(1)}, u32[]{:S(2)}) copy-start(f32[512,128]{1,0:T(8,128)S(1)} %fusion.10) | copy-start | bytes 786436
  183.5 106.1 %all-to-all-start.2 = ((bf16[32,128,1024]{1,2,0:T(8,128)(2,1)}), bf16[32,128,1024]{1,2,0:T(8,128)(2,1)}, u32[]{:S(2)}, u32[]{:S(2)}) async-start(bf16[32,128,1024]{1,2,0:T(8,128)(2,1)} %stack.2), calls=%async_computation.2 | async-start | bytes 16777216 | tf_op jit(solution)/shard_map/all_to_all | solution.py:51
  307.4 6.4 %copy-start.1 = (bf16[768,512]{1,0:T(8,128)(2,1)S(1)}, bf16[768,512]{1,0:T(8,128)(2,1)}, u32[]{:S(2)}) copy-start(bf16[768,512]{1,0:T(8,128)(2,1)} %param.21) | copy-start | bytes 2359300
Sparse Core Ops, SparseCore 0:
  10.8 49.7 all-gather.2
  135.0 39.8 all-gather.4
